TPU v7x, 32 devices: a whole 2x2x4 slice. The times are simulated.
32 devices in a mesh: sp: 8 (over z, x), tp: 4 (over y, core).
Axes of the slice: x: 2, y: 2, z: 4, core: 2. Of those that a mesh axis runs over, the one named last changes fastest.
Arguments:
- queries: bfloat16 [1024, 2048], P('sp', 'tp'), may hold values from -18 to 90
- projected_key_rows: bfloat16 [1024, 1024], P('sp', 'tp'), may hold values from -18 to 90
- projected_value_rows: bfloat16 [1024, 1024], P('sp', 'tp'), may hold values from -6 to 6
- query_gain: float32 [64], replicated, may hold values from 1 to 6
- key_norm_gain: float32 [64], replicated, may hold values from 1 to 6
- residual: bfloat16 [1024, 2048], P('sp', 'tp'), may hold values from -54 to 54
- out_weight: bfloat16 [2048, 2048], P('tp'), may hold values from -1 to 1
- norm_gain: float32 [2048], P('tp'), may hold values from 0.28 to 4.68
- expert_ids: int32 [1024, 2], P('sp'), may hold values from 0 to 7, as said below
- route_weights: float32 [1024, 2], P('sp'), may hold values from 0.2 to 1
- gate_weight: bfloat16 [8, 2048, 4096], P('sp', None, 'tp'), may hold values from -0.125 to 0.125
- up_weight: bfloat16 [8, 2048, 4096], P('sp', None, 'tp'), may hold values from -0.125 to 0.125
- down_weight: bfloat16 [8, 4096, 2048], P('sp', 'tp'), may hold values from -0.25 to 0.25
- final_gain: float32 [2048], P('tp'), may hold values from 0.1 to 1.9
Outputs:
- layer_out: bfloat16 [1024, 2048], P('sp', 'tp')
Inputs may be any that keep to these rules, and one draw needn't show every extreme that they name: `expert_ids`: each row names two different experts of one group, the group of expert e being e // 4. In every aligned block of 128 rows each group is named by the same number of rows, no expert is named by more than 64 rows, one expert of every group is named by exactly 64 rows, and one expert is named by 64 rows of every block.
All inputs are finite; a program needn't handle non-finite values.
Results may differ from a plain program's by a relative error of at most 0.019.
The roundings to bfloat16 on the way count: a program that leaves them out, or rounds other values in their place, can miss the bound.
Values may be sent and summed in bfloat16 or wider, within the bound.
A program may use at most 64 MiB of HBM per device.

v0:
```python
from functools import reduce
import jax
import jax.numpy as jnp
from jax import lax
from jax.sharding import PartitionSpec as P

D = 2048
HEAD_DIM = 64
GRID_W = 64
TOPK = 2
theta_base = 10000.0
norm_epsilon = 1e-06
residual_scale = 8.0**0.25
far_below = -1e30


def rope_line(halves, angles):
    pair_count = angles.shape[-1]
    first_half = halves[..., :pair_count]
    second_half = halves[..., pair_count:]
    cosine = jnp.cos(angles)[:, None, :]
    sine_part = jnp.sin(angles)[:, None, :]
    return jnp.concatenate(
        [
            first_half * cosine - second_half * sine_part,
            first_half * sine_part + second_half * cosine,
        ],
        -1,
    )


def rotary_over_grid(rows_by_head, token_positions):
    head_size = rows_by_head.shape[-1]
    frequency = theta_base ** (
        -jnp.arange(0, head_size // 2, 2, dtype=jnp.float32) / (head_size // 2)
    )
    grid_row = (token_positions // GRID_W).astype(jnp.float32)
    grid_col = (token_positions % GRID_W).astype(jnp.float32)
    row_part = rope_line(
        rows_by_head[..., : head_size // 2], grid_row[:, None] * frequency[None, :]
    )
    col_part = rope_line(
        rows_by_head[..., head_size // 2 :], grid_col[:, None] * frequency[None, :]
    )
    return jnp.concatenate([row_part, col_part], -1)


def normalize_heads(token_rows, gain_row, head_count):
    shaped = token_rows.astype(jnp.float32).reshape(token_rows.shape[0], head_count, -1)
    scaled = shaped * lax.rsqrt(jnp.mean(shaped * shaped, -1, keepdims=True) + norm_epsilon)
    return scaled * gain_row[None, None, :]


def norm_features(feature_rows, gain_row, feature_total):
    row_sums = jnp.sum(feature_rows, 0)
    squares = jnp.sum(feature_rows * feature_rows, 0)
    row_sums, squares = lax.psum((row_sums, squares), "tp")
    center = row_sums / feature_total
    spread = squares / feature_total - center * center
    return (
        (feature_rows - center[None, :])
        * lax.rsqrt(spread + norm_epsilon)[None, :]
        * gain_row[:, None]
    )


def per_device(
    queries,
    projected_key_rows,
    projected_value_rows,
    query_gain,
    key_norm_gain,
    residual,
    out_weight,
    norm_gain,
    expert_ids,
    route_weights,
    gate_weight,
    up_weight,
    down_weight,
    final_gain,
):
    token_count = queries.shape[0]
    query_heads = queries.shape[1] // HEAD_DIM
    key_heads = projected_key_rows.shape[1] // HEAD_DIM
    queries_per_group = query_heads // key_heads
    token_positions = lax.axis_index("sp") * token_count + jnp.arange(token_count, dtype=jnp.int32)
    queries_after_rotation = rotary_over_grid(
        normalize_heads(queries, query_gain, query_heads), token_positions
    ).astype(jnp.bfloat16)
    keys_after_rotation = rotary_over_grid(
        normalize_heads(projected_key_rows, key_norm_gain, key_heads), token_positions
    ).astype(jnp.bfloat16)
    packed = jnp.concatenate(
        [keys_after_rotation, projected_value_rows.reshape(token_count, key_heads, HEAD_DIM)], -1
    ).reshape(token_count, key_heads * 2 * HEAD_DIM)
    grouped_query_heads = (
        queries_after_rotation.reshape(token_count, key_heads, queries_per_group, HEAD_DIM)
        .transpose(1, 2, 0, 3)
        .reshape(key_heads, queries_per_group * token_count, HEAD_DIM)
    )
    score_scale = HEAD_DIM ** (-0.5)
    query_total = queries_per_group * token_count
    section = lax.all_gather(packed, "sp", axis=0, tiled=True)
    running_max = jnp.full((key_heads, query_total), far_below, jnp.float32)
    opened = section.reshape(section.shape[0], key_heads, 2 * HEAD_DIM)
    scores = (
        jnp.einsum(
            "hqd,khd->hqk",
            grouped_query_heads,
            opened[:, :, :HEAD_DIM],
            preferred_element_type=jnp.float32,
        )
        * score_scale
    )
    new_peak = jnp.maximum(running_max, jnp.max(scores, -1))
    weights = jnp.exp(scores - new_peak[:, :, None])
    running_sum = jnp.sum(weights, -1)
    running_out = jnp.einsum(
        "hqk,khd->hqd",
        weights.astype(jnp.bfloat16),
        opened[:, :, HEAD_DIM:],
        preferred_element_type=jnp.float32,
    )
    running_max, running_sum, running_out = (new_peak, running_sum, running_out)
    attended = (running_out / running_sum[:, :, None]).astype(jnp.bfloat16)
    attended = (
        attended.reshape(key_heads, queries_per_group, token_count, HEAD_DIM)
        .transpose(2, 0, 1, 3)
        .reshape(token_count, query_heads * HEAD_DIM)
    )
    local_width = residual.shape[1]
    columns = out_weight
    mixed_rows = lax.psum_scatter(
        lax.dot_general(
            columns, attended, (((0,), (1,)), ((), ())), preferred_element_type=jnp.float32
        ).astype(jnp.bfloat16),
        "tp",
        scatter_dimension=0,
        tiled=True,
    ).astype(jnp.float32)
    pre_norm = residual_scale * residual.astype(jnp.float32).T + mixed_rows
    normed = norm_features(pre_norm, norm_gain, D).astype(jnp.bfloat16)
    expert_count = lax.axis_size("sp")
    capacity = 4 * token_count // expert_count
    row_total = expert_count * capacity
    flat_ids = expert_ids.reshape(-1)
    marked = (flat_ids[:, None] == jnp.arange(expert_count, dtype=jnp.int32)[None, :]).astype(
        jnp.int32
    )
    earlier = jnp.cumsum(marked, 0) - marked
    places = (flat_ids * capacity + jnp.sum(earlier * marked, 1)).reshape(token_count, TOPK)
    lane_index = jnp.arange(row_total, dtype=jnp.int32)
    selectors = [
        (places[:, route_rank : route_rank + 1] == lane_index[None, :]).astype(jnp.bfloat16)
        for route_rank in range(TOPK)
    ]
    dispatch = reduce(jnp.add, selectors)
    gate_local = gate_weight[0]
    up_local = up_weight[0]
    down_local = down_weight[0]
    outgoing = lax.dot_general(
        dispatch, normed, (((0,), (1,)), ((), ())), preferred_element_type=jnp.float32
    ).astype(jnp.bfloat16)
    arrived = lax.all_to_all(
        outgoing.reshape(expert_count, capacity, local_width),
        "sp",
        split_axis=0,
        concat_axis=0,
        tiled=True,
    ).reshape(row_total, local_width)
    section = lax.all_gather(arrived, "tp", axis=1, tiled=True)
    gate_sum = jnp.dot(section, gate_local, preferred_element_type=jnp.float32)
    up_sum = jnp.dot(section, up_local, preferred_element_type=jnp.float32)
    hidden = (jax.nn.silu(gate_sum) * up_sum).astype(jnp.bfloat16)
    columns = down_local
    expert_out = lax.psum_scatter(
        lax.dot_general(
            columns, hidden, (((0,), (1,)), ((), ())), preferred_element_type=jnp.float32
        ).astype(jnp.bfloat16),
        "tp",
        scatter_dimension=0,
        tiled=True,
    )
    returned = lax.all_to_all(
        expert_out.reshape(local_width, expert_count, capacity),
        "sp",
        split_axis=1,
        concat_axis=1,
        tiled=True,
    ).reshape(local_width, row_total)
    combined = jnp.zeros((local_width, token_count), jnp.float32)
    for route_rank in range(TOPK):
        chosen = lax.dot_general(
            returned,
            selectors[route_rank],
            (((1,), (1,)), ((), ())),
            preferred_element_type=jnp.float32,
        )
        combined = combined + chosen * route_weights[:, route_rank][None, :]
    second_sum = residual_scale * normed.astype(jnp.float32) + combined
    return norm_features(second_sum, final_gain, D).T.astype(jnp.bfloat16)


def solution(mesh):
    in_specs = (
        P("sp", "tp"),
        P("sp", "tp"),
        P("sp", "tp"),
        P(),
        P(),
        P("sp", "tp"),
        P("tp", None),
        P("tp"),
        P("sp", None),
        P("sp", None),
        P("sp", None, "tp"),
        P("sp", None, "tp"),
        P("sp", "tp", None),
        P("tp"),
    )
    out_specs = P("sp", "tp")
    return jax.shard_map(
        per_device, mesh=mesh, in_specs=in_specs, out_specs=out_specs, check_vma=False
    )
```

profile of v0, /device:TPU:0, one launch (start us, length us, event | category | flops | bytes accessed | tf_op | source)
XLA Modules:
  0.0 209.7 jit_solution(3007069951881743205)
XLA Ops:
  6.6 1.1 copy.42
  7.7 0.7 fusion.43
  8.5 0.1 multiply_cosine_fusion
  8.7 1.0 copy.43
  9.7 0.6 copy-done.2
  10.4 1.0 copy.40
  11.5 0.7 fusion.38
  12.3 40.3 %all-gather.3.cloned.1.call-done = bf16[1024,512]{0,1:T(8,128)(2,1)} async-done(((bf16[128,512]{0,1:T(8,128)(2,1)}), bf16[1024,512]{0,1:T(8,128)(2,1)}) %all-gather.3.cloned.1.call-update) | async-done | bytes 1048592 | tf_op jit(solution)/shard_map/all_gather | solution.py:104
  52.6 2.0 multiply_reduce_fusion
  54.6 0.9 fusion.6
  55.5 0.9 fusion.29
  56.5 1.3 fusion.14
  58.0 0.1 eq.62
  58.1 0.1 eq.58
  58.3 0.6 reduce-window.6
  58.9 0.2 slice_reduce_fusion
  59.2 0.1 reduce_sum.80
  59.5 19.2 %reduce-scatter.3.cloned.1.call-done = bf16[512,128]{0,1:T(8,128)(2,1)} async-done(((bf16[2048,128]{0,1:T(8,128)(2,1)}), bf16[512,128]{0,1:T(8,128)(2,1)}) %reduce-scatter.3.cloned.1.call-update) | async-done | bytes 131088 | tf_op jit(solution)/shard_map/reduce_scatter | solution.py:134
  78.7 1.0 fusion.41
  79.7 5.8 %all-reduce.1 = (f32[128]{0:T(128)S(1)}, f32[128]{0:T(128)S(1)}) all-reduce(f32[128]{0:T(128)S(1)} %get-tuple-element.8, f32[128]{0:T(128)S(1)} %get-tuple-element.7), channel_id=1, replica_groups=mesh['sp'=8,'tp'=4] {'tp'}, use_global_device_ids=true, to_apply=%region_8.9 | all-reduce | flops 256 | bytes 2048 | tf_op jit(solution)/shard_map/psum | solution.py:57
  85.5 1.3 convolution_convert_fusion.1
  86.8 19.8 %all_to_all.10 = bf16[8,64,512]{2,1,0:T(8,128)(2,1)} all-to-all(bf16[8,64,512]{2,1,0:T(8,128)(2,1)S(1)} %bitcast.97), channel_id=1, replica_groups=mesh['sp'=8,'tp'=4] {'sp'}, dimensions={0} | all-to-all | bytes 1048576 | tf_op jit(solution)/shard_map/all_to_all | solution.py:165
  106.7 20.8 %all-gather.5.cloned.1.call-done = bf16[512,2048]{1,0:T(8,128)(2,1)} async-done(((bf16[512,512]{1,0:T(8,128)(2,1)}), bf16[512,2048]{1,0:T(8,128)(2,1)}) %all-gather.5.cloned.1.call-update) | async-done | bytes 2097168 | tf_op jit(solution)/shard_map/all_gather | solution.py:172
  127.5 6.5 %fusion.4 = f32[512,1024]{1,0:T(8,128)} fusion(bf16[512,2048]{1,0:T(8,128)(2,1)} %all-gather.5.cloned.1.call-done, bf16[1,2048,1024]{2,1,0:T(8,128)(2,1)} %param.24), kind=kOutput, calls=%fused_computation.4 | convolution fusion | flops 2147483648 | bytes 8388608 | tf_op jit(solution)/shard_map/dot_general | solution.py:173
  134.0 10.6 %fusion.11 = bf16[2048,512]{0,1:T(8,128)(2,1)} fusion(bf16[1,1024,2048]{2,1,0:T(8,128)(2,1)} %param.26, f32[512,1024]{1,0:T(8,128)} %fusion.4, bf16[512,2048]{1,0:T(8,128)(2,1)} %all-gather.5.cloned.1.call-done, bf16[1,2048,1024]{2,1,0:T(8,128)(2,1)} %param.25), kind=kOutput, calls=%fused_computation.11 | convolution fusion | flops 4299161600 | bytes 14680064 | tf_op jit(solution)/shard_map/dot_general | solution.py:178
  144.6 31.3 %reduce-scatter.5.cloned.1.call-done = bf16[512,512]{0,1:T(8,128)(2,1)} async-done(((bf16[2048,512]{0,1:T(8,128)(2,1)}), bf16[512,512]{0,1:T(8,128)(2,1)}) %reduce-scatter.5.cloned.1.call-update) | async-done | bytes 524304 | tf_op jit(solution)/shard_map/reduce_scatter | solution.py:177
  175.9 5.5 %all-to-all-start.1 = ((bf16[512,8,64]{0,2,1:T(8,128)(2,1)}), bf16[512,8,64]{0,2,1:T(8,128)(2,1)S(1)}, u32[]{:S(2)}, u32[]{:S(2)}) async-start(bf16[512,8,64]{0,2,1:T(8,128)(2,1)} %bitcast.96), calls=%async_computation.3 | async-start | bytes 1048576 | tf_op jit(solution)/shard_map/all_to_all | solution.py:185
  181.5 14.3 %all-to-all-done.1 = bf16[512,8,64]{0,2,1:T(8,128)(2,1)S(1)} async-done(((bf16[512,8,64]{0,2,1:T(8,128)(2,1)}), bf16[512,8,64]{0,2,1:T(8,128)(2,1)S(1)}, u32[]{:S(2)}, u32[]{:S(2)}) %all-to-all-start.1) | async-done | bytes 524320 | tf_op jit(solution)/shard_map/all_to_all | solution.py:185
  195.8 0.3 convolution_multiply_fusion.1
  196.1 0.4 fusion.65
  196.5 5.9 %all-reduce = (f32[128]{0:T(128)S(1)}, f32[128]{0:T(128)S(1)}) all-reduce(f32[128]{0:T(128)S(1)} %get-tuple-element.6, f32[128]{0:T(128)S(1)} %get-tuple-element.5), channel_id=1, replica_groups=mesh['sp'=8,'tp'=4] {'tp'}, use_global_device_ids=true, to_apply=%region_16.17 | all-reduce | flops 256 | bytes 2048 | tf_op jit(solution)/shard_map/psum | solution.py:57
  202.4 0.8 fusion.47
  (50 shorter events, 0.8 us)
Async XLA Ops:
  6.5 50.0 %copy-start = (bf16[512,2048]{1,0:T(8,128)(2,1)S(1)}, bf16[512,2048]{1,0:T(8,128)(2,1)}, u32[]{:S(2)}) copy-start(bf16[512,2048]{1,0:T(8,128)(2,1)} %param.20) | copy-start | bytes 6291460
  6.5 46.1 %all-gather.3.cloned.1.call-start = ((), (), s32[]{:S(2)}) async-start(), calls=%async_computation.4 | async-start | bytes 1179648 | tf_op jit(solution)/shard_map/all_gather | solution.py:104
  9.7 0.7 copy-start.2
  10.3 68.3 %reduce-scatter.3.cloned.1.call-start = ((), (), s32[]{:S(2)}) async-start(), calls=%async_computation.5 | async-start | bytes 655360 | tf_op jit(solution)/shard_map/reduce_scatter | solution.py:134
  52.6 2.9 %copy-start.1 = (bf16[1024,512]{0,1:T(8,128)(2,1)S(1)}, bf16[1024,512]{0,1:T(8,128)(2,1)}, u32[]{:S(2)}) copy-start(bf16[1024,512]{0,1:T(8,128)(2,1)} %all-gather.3.cloned.1.call-done) | copy-start | bytes 3145732
  55.5 2.4 %copy-start.5 = (s32[128,2]{0,1:T(2,128)S(1)}, s32[128,2]{0,1:T(2,128)}, u32[]{:S(2)}) copy-start(s32[128,2]{0,1:T(2,128)} %param.22) | copy-start | bytes 3076
  55.5 23.2 %copy-start.3 = (bf16[128,512]{1,0:T(8,128)(2,1)S(1)}, bf16[128,512]{1,0:T(8,128)(2,1)}, u32[]{:S(2)}) copy-start(bf16[128,512]{1,0:T(8,128)(2,1)} %param.19) | copy-start | bytes 393220
  55.5 30.0 %copy-start.8 = (f32[512]{0:T(512)S(1)}, f32[512]{0:T(512)}, u32[]{:S(2)}) copy-start(f32[512]{0:T(512)} %param.21) | copy-start | bytes 6148
  57.8 69.7 %all-gather.5.cloned.1.call-start = ((), (), s32[]{:S(2)}) async-start(), calls=%async_computation.6 | async-start | bytes 2621440 | tf_op jit(solution)/shard_map/all_gather | solution.py:172
  106.7 69.3 %reduce-scatter.5.cloned.1.call-start = ((), (), s32[]{:S(2)}) async-start(), calls=%async_computation.7 | async-start | bytes 2621440 | tf_op jit(solution)/shard_map/reduce_scatter | solution.py:177
  134.0 47.4 %copy-start.7 = (f32[128,2]{0,1:T(2,128)S(1)}, f32[128,2]{0,1:T(2,128)}, u32[]{:S(2)}) copy-start(f32[128,2]{0,1:T(2,128)} %param.23) | copy-start | bytes 3076
  134.0 62.0 %copy-start.4 = (bf16[512,128]{0,1:T(8,128)(2,1)S(1)}, bf16[512,128]{0,1:T(8,128)(2,1)}, u32[]{:S(2)}) copy-start(bf16[512,128]{0,1:T(8,128)(2,1)} %reduce-scatter.3.cloned.1.call-done) | copy-start | bytes 393220
  144.6 57.8 %copy-start.6 = (f32[512]{0:T(512)S(1)}, f32[512]{0:T(512)}, u32[]{:S(2)}) copy-start(f32[512]{0:T(512)} %param.27) | copy-start | bytes 6148
  175.9 19.8 %all-to-all-start.1 = ((bf16[512,8,64]{0,2,1:T(8,128)(2,1)}), bf16[512,8,64]{0,2,1:T(8,128)(2,1)S(1)}, u32[]{:S(2)}, u32[]{:S(2)}) async-start(bf16[512,8,64]{0,2,1:T(8,128)(2,1)} %bitcast.96), calls=%async_computation.3 | async-start | bytes 1048576 | tf_op jit(solution)/shard_map/all_to_all | solution.py:185
Sparse Core Ops, SparseCore 0:
  10.5 42.1 all-gather.2
  57.9 20.6 reduce-scatter.2
  106.8 20.7 all-gather.4
  144.7 31.1 reduce-scatter.4
where the time goes:
time: 210 us
  waiting for transfers between devices  126 us (60%)
  blocking collectives  31.5 us (15%)
  matrix products  23.2 us (11%)
  between operations  13.4 us (6%)
  starting transfers between devices  5.64 us (3%)
  other arithmetic  5.31 us (3%)
  local copies, waits for them, and re-layouts  4.61 us (2%)
    all_gather x1, waiting for transfers between devices, per_device(): section = lax.all_gather(packed, 'sp', axis=0, tiled=True)  40.3 us
    reduce_scatter x1, waiting for transfers between devices, per_device(): lax.psum_scatter(lax.dot_general(columns, hidden, (((0,), (1,)), ((), ())...  31.3 us
    all_gather x1, waiting for transfers between devices, per_device(): section = lax.all_gather(arrived, 'tp', axis=1, tiled=True)  20.8 us
    all_to_all x1, blocking collectives, per_device(): lax.all_to_all(outgoing.reshape(expert_count, capacity, local_width), 'sp...  19.8 us
    reduce_scatter x1, waiting for transfers between devices, per_device(): lax.psum_scatter(lax.dot_general(columns, attended, (((0,), (1,)), ((), (...  19.2 us
    all_to_all x1, waiting for transfers between devices, per_device(): lax.all_to_all(expert_out.reshape(local_width, expert_count, capacity), '...  14.3 us
    psum x2, blocking collectives, norm_features(): row_sums, squares = lax.psum((row_sums, squares), 'tp')  11.7 us
    dot_general x1, matrix products, per_device(): lax.dot_general(columns, hidden, (((0,), (1,)), ((), ())), preferred_elem...  10.6 us
  transfers between devices with their start and end apart: 5, of which 5 were waited for; matrix products, arithmetic and copies ran while one was open for 2% of the time, Pallas kernels for 0%

commit v1 on v0

--- a/solution.py
+++ b/solution.py
@@ -182,12 +182,20 @@
         scatter_dimension=0,
         tiled=True,
     )
-    returned = lax.all_to_all(
-        expert_out.reshape(local_width, expert_count, capacity),
-        "sp",
-        split_axis=1,
-        concat_axis=1,
-        tiled=True,
+    returned = jnp.concatenate(
+        lax.all_to_all(
+            jnp.stack(
+                jnp.split(
+                    expert_out.reshape(local_width, expert_count, capacity),
+                    lax.axis_size("sp"),
+                    axis=1,
+                )
+            ),
+            "sp",
+            0,
+            0,
+        ),
+        axis=1,
     ).reshape(local_width, row_total)
     combined = jnp.zeros((local_width, token_count), jnp.float32)
     for route_rank in range(TOPK):

time: 210 us -> 222 us (1.057)
  local copies, waits for them, and re-layouts: 4.61 us -> 16.3 us
    unnamed x22 -> x29, local copies, waits for them, and re-layouts: 3.87 us -> 14.1 us
where the time goes in v1:
time: 222 us; the launch traced here: 221 us
  waiting for transfers between devices  126 us (57%)
  blocking collectives  31.5 us (14%)
  matrix products  23.2 us (10%)
  local copies, waits for them, and re-layouts  16.3 us (7%)
  between operations  13.4 us (6%)
  starting transfers between devices  5.64 us (3%)
  other arithmetic  5.31 us (2%)
    all_gather x1, waiting for transfers between devices, per_device(): section = lax.all_gather(packed, 'sp', axis=0, tiled=True)  40.3 us
    reduce_scatter x1, waiting for transfers between devices, per_device(): lax.psum_scatter(lax.dot_general(columns, hidden, (((0,), (1,)), ((), ())...  31.3 us
    all_gather x1, waiting for transfers between devices, per_device(): section = lax.all_gather(arrived, 'tp', axis=1, tiled=True)  20.8 us
    all_to_all x1, blocking collectives, per_device(): lax.all_to_all(outgoing.reshape(expert_count, capacity, local_width), 'sp...  19.8 us
    reduce_scatter x1, waiting for transfers between devices, per_device(): lax.psum_scatter(lax.dot_general(columns, attended, (((0,), (1,)), ((), (...  19.2 us
    all_to_all x1, waiting for transfers between devices, per_device(): lax.all_to_all(jnp.stack(jnp.split(expert_out.reshape(local_width, expert...  14.3 us
    unnamed x29, local copies, waits for them, and re-layouts  14.1 us
    psum x2, blocking collectives, norm_features(): row_sums, squares = lax.psum((row_sums, squares), 'tp')  11.7 us
  transfers between devices with their start and end apart: 5, of which 5 were waited for; matrix products, arithmetic and copies ran while one was open for 2% of the time, Pallas kernels for 0%

profile of v1, /device:TPU:0, one launch (start us, length us, event | category | flops | bytes accessed | tf_op | source)
XLA Modules:
  0.0 221.4 jit_solution(9057989226252093809)
XLA Ops:
  6.6 1.1 copy.42
  7.7 0.7 fusion.43
  8.7 1.0 copy.43
  9.7 0.6 copy-done.2
  10.4 1.0 copy.40
  11.5 0.7 fusion.38
  12.3 40.3 %all-gather.3.cloned.1.call-done = bf16[1024,512]{0,1:T(8,128)(2,1)} async-done(((bf16[128,512]{0,1:T(8,128)(2,1)}), bf16[1024,512]{0,1:T(8,128)(2,1)}) %all-gather.3.cloned.1.call-update) | async-done | bytes 1048592 | tf_op jit(solution)/shard_map/all_gather | solution.py:104
  52.6 2.0 multiply_reduce_fusion
  54.6 0.9 fusion.6
  55.5 0.9 fusion.29
  56.5 1.3 fusion.14
  59.5 19.2 %reduce-scatter.3.cloned.1.call-done = bf16[512,128]{0,1:T(8,128)(2,1)} async-done(((bf16[2048,128]{0,1:T(8,128)(2,1)}), bf16[512,128]{0,1:T(8,128)(2,1)}) %reduce-scatter.3.cloned.1.call-update) | async-done | bytes 131088 | tf_op jit(solution)/shard_map/reduce_scatter | solution.py:134
  78.7 1.0 fusion.41
  79.7 5.8 %all-reduce.1 = (f32[128]{0:T(128)S(1)}, f32[128]{0:T(128)S(1)}) all-reduce(f32[128]{0:T(128)S(1)} %get-tuple-element.8, f32[128]{0:T(128)S(1)} %get-tuple-element.7), channel_id=1, replica_groups=mesh['sp'=8,'tp'=4] {'tp'}, use_global_device_ids=true, to_apply=%region_8.9 | all-reduce | flops 256 | bytes 2048 | tf_op jit(solution)/shard_map/psum | solution.py:57
  85.5 1.3 convolution_convert_fusion.1
  86.8 19.8 %all_to_all.10 = bf16[8,64,512]{2,1,0:T(8,128)(2,1)} all-to-all(bf16[8,64,512]{2,1,0:T(8,128)(2,1)S(1)} %bitcast.138), channel_id=1, replica_groups=mesh['sp'=8,'tp'=4] {'sp'}, dimensions={0} | all-to-all | bytes 1048576 | tf_op jit(solution)/shard_map/all_to_all | solution.py:165
  106.7 20.8 %all-gather.5.cloned.1.call-done = bf16[512,2048]{1,0:T(8,128)(2,1)} async-done(((bf16[512,512]{1,0:T(8,128)(2,1)}), bf16[512,2048]{1,0:T(8,128)(2,1)}) %all-gather.5.cloned.1.call-update) | async-done | bytes 2097168 | tf_op jit(solution)/shard_map/all_gather | solution.py:172
  127.5 6.5 %fusion.4 = f32[512,1024]{1,0:T(8,128)} fusion(bf16[512,2048]{1,0:T(8,128)(2,1)} %all-gather.5.cloned.1.call-done, bf16[1,2048,1024]{2,1,0:T(8,128)(2,1)} %param.24), kind=kOutput, calls=%fused_computation.4 | convolution fusion | flops 2147483648 | bytes 8388608 | tf_op jit(solution)/shard_map/dot_general | solution.py:173
  134.0 10.5 %fusion.11 = bf16[2048,512]{0,1:T(8,128)(2,1)} fusion(bf16[1,1024,2048]{2,1,0:T(8,128)(2,1)} %param.26, f32[512,1024]{1,0:T(8,128)} %fusion.4, bf16[512,2048]{1,0:T(8,128)(2,1)} %all-gather.5.cloned.1.call-done, bf16[1,2048,1024]{2,1,0:T(8,128)(2,1)} %param.25), kind=kOutput, calls=%fused_computation.11 | convolution fusion | flops 4299161600 | bytes 14680064 | tf_op jit(solution)/shard_map/dot_general | solution.py:178
  144.6 31.3 %reduce-scatter.5.cloned.1.call-done = bf16[512,512]{0,1:T(8,128)(2,1)} async-done(((bf16[2048,512]{0,1:T(8,128)(2,1)}), bf16[512,512]{0,1:T(8,128)(2,1)}) %reduce-scatter.5.cloned.1.call-update) | async-done | bytes 524304 | tf_op jit(solution)/shard_map/reduce_scatter | solution.py:177
  175.9 1.5 fusion.61
  177.4 1.5 fusion.60
  178.8 1.5 fusion.59
  180.3 1.5 fusion.58
  181.8 1.5 fusion.57
  183.2 1.5 fusion.56
  184.7 1.5 fusion.55
  186.2 1.5 fusion.54
  187.6 5.5 %all-to-all-start.1 = ((bf16[8,512,1,64]{1,3,2,0:T(8,128)(2,1)}), bf16[8,512,1,64]{1,3,2,0:T(8,128)(2,1)S(1)}, u32[]{:S(2)}, u32[]{:S(2)}) async-start(bf16[8,512,1,64]{1,3,2,0:T(8,128)(2,1)} %fusion.54), calls=%async_computation.3 | async-start | bytes 1048576 | tf_op jit(solution)/shard_map/all_to_all | solution.py:186
  193.2 14.3 %all-to-all-done.1 = bf16[8,512,1,64]{1,3,2,0:T(8,128)(2,1)S(1)} async-done(((bf16[8,512,1,64]{1,3,2,0:T(8,128)(2,1)}), bf16[8,512,1,64]{1,3,2,0:T(8,128)(2,1)S(1)}, u32[]{:S(2)}, u32[]{:S(2)}) %all-to-all-start.1) | async-done | bytes 524320 | tf_op jit(solution)/shard_map/all_to_all | solution.py:186
  208.1 5.9 %all-reduce = (f32[128]{0:T(128)S(1)}, f32[128]{0:T(128)S(1)}) all-reduce(f32[128]{0:T(128)S(1)} %get-tuple-element.6, f32[128]{0:T(128)S(1)} %get-tuple-element.5), channel_id=1, replica_groups=mesh['sp'=8,'tp'=4] {'tp'}, use_global_device_ids=true, to_apply=%region_16.17 | all-reduce | flops 256 | bytes 2048 | tf_op jit(solution)/shard_map/psum | solution.py:57
  214.1 0.8 fusion.47
  (58 shorter events, 2.9 us)
Async XLA Ops:
  6.5 50.0 %copy-start = (bf16[512,2048]{1,0:T(8,128)(2,1)S(1)}, bf16[512,2048]{1,0:T(8,128)(2,1)}, u32[]{:S(2)}) copy-start(bf16[512,2048]{1,0:T(8,128)(2,1)} %param.20) | copy-start | bytes 6291460
  6.5 46.1 %all-gather.3.cloned.1.call-start = ((), (), s32[]{:S(2)}) async-start(), calls=%async_computation.4 | async-start | bytes 1179648 | tf_op jit(solution)/shard_map/all_gather | solution.py:104
  9.7 0.7 copy-start.2
  10.3 68.3 %reduce-scatter.3.cloned.1.call-start = ((), (), s32[]{:S(2)}) async-start(), calls=%async_computation.5 | async-start | bytes 655360 | tf_op jit(solution)/shard_map/reduce_scatter | solution.py:134
  52.6 2.9 %copy-start.1 = (bf16[1024,512]{0,1:T(8,128)(2,1)S(1)}, bf16[1024,512]{0,1:T(8,128)(2,1)}, u32[]{:S(2)}) copy-start(bf16[1024,512]{0,1:T(8,128)(2,1)} %all-gather.3.cloned.1.call-done) | copy-start | bytes 3145732
  55.5 2.4 %copy-start.5 = (s32[128,2]{0,1:T(2,128)S(1)}, s32[128,2]{0,1:T(2,128)}, u32[]{:S(2)}) copy-start(s32[128,2]{0,1:T(2,128)} %param.22) | copy-start | bytes 3076
  55.5 23.2 %copy-start.3 = (bf16[128,512]{1,0:T(8,128)(2,1)S(1)}, bf16[128,512]{1,0:T(8,128)(2,1)}, u32[]{:S(2)}) copy-start(bf16[128,512]{1,0:T(8,128)(2,1)} %param.19) | copy-start | bytes 393220
  55.5 30.0 %copy-start.8 = (f32[512]{0:T(512)S(1)}, f32[512]{0:T(512)}, u32[]{:S(2)}) copy-start(f32[512]{0:T(512)} %param.21) | copy-start | bytes 6148
  57.8 69.7 %all-gather.5.cloned.1.call-start = ((), (), s32[]{:S(2)}) async-start(), calls=%async_computation.6 | async-start | bytes 2621440 | tf_op jit(solution)/shard_map/all_gather | solution.py:172
  106.7 69.3 %reduce-scatter.5.cloned.1.call-start = ((), (), s32[]{:S(2)}) async-start(), calls=%async_computation.7 | async-start | bytes 2621440 | tf_op jit(solution)/shard_map/reduce_scatter | solution.py:177
  144.6 48.6 %copy-start.7 = (f32[128,2]{0,1:T(2,128)S(1)}, f32[128,2]{0,1:T(2,128)}, u32[]{:S(2)}) copy-start(f32[128,2]{0,1:T(2,128)} %param.23) | copy-start | bytes 3076
  144.6 63.2 %copy-start.4 = (bf16[512,128]{0,1:T(8,128)(2,1)S(1)}, bf16[512,128]{0,1:T(8,128)(2,1)}, u32[]{:S(2)}) copy-start(bf16[512,128]{0,1:T(8,128)(2,1)} %reduce-scatter.3.cloned.1.call-done) | copy-start | bytes 393220
  144.6 69.5 %copy-start.6 = (f32[512]{0:T(512)S(1)}, f32[512]{0:T(512)}, u32[]{:S(2)}) copy-start(f32[512]{0:T(512)} %param.27) | copy-start | bytes 6148
  187.6 19.8 %all-to-all-start.1 = ((bf16[8,512,1,64]{1,3,2,0:T(8,128)(2,1)}), bf16[8,512,1,64]{1,3,2,0:T(8,128)(2,1)S(1)}, u32[]{:S(2)}, u32[]{:S(2)}) async-start(bf16[8,512,1,64]{1,3,2,0:T(8,128)(2,1)} %fusion.54), calls=%async_computation.3 | async-start | bytes 1048576 | tf_op jit(solution)/shard_map/all_to_all | solution.py:186
Sparse Core Ops, SparseCore 0:
  10.5 42.1 all-gather.2
  57.9 20.6 reduce-scatter.2
  106.8 20.7 all-gather.4
  144.7 31.1 reduce-scatter.4
